TPU v7x, 32 devices: a whole 2x2x4 slice. The times are simulated.
32 devices in a mesh: grp: 2 (over y), fs: 4 (over z), tp: 4 (over x, core).
Axes of the slice: x: 2, y: 2, z: 4, core: 2. Of those that a mesh axis runs over, the one named last changes fastest.
Arguments:
- tokens: bfloat16 [4096, 2048], P(('grp', 'fs'), 'tp'), parts along dimension 0, may hold values from -6 to 6
- first_gain: bfloat16 [2048], replicated, may hold values from 0.099609375 to 1.8984375
- u_proj: bfloat16 [2048, 1024], P('fs', 'tp'), may hold values from -0.125 to 0.125
- v_proj: bfloat16 [2048, 1024], P('fs', 'tp'), may hold values from -0.125 to 0.125
- group_gain: bfloat16 [8, 128], P('tp'), may hold values from 0.099609375 to 1.8984375
- spatial: bfloat16 [8, 128, 128], P('tp'), may hold values from -0.5 to 0.5
- spatial_bias: bfloat16 [8, 128], P('tp'), may hold values from 0.099609375 to 1.8984375
- mix_proj: bfloat16 [1024, 2048], P('fs', 'tp'), may hold values from -0.1875 to 0.1875
- second_gain: bfloat16 [2048], replicated, may hold values from 0.099609375 to 1.8984375
- up_proj: bfloat16 [2048, 8192], P('fs', 'tp'), may hold values from -0.125 to 0.125
- down_proj: bfloat16 [8192, 2048], P('tp', 'fs'), may hold values from -0.0625 to 0.0625
Outputs:
- layer_out: bfloat16 [4096, 2048], P(('grp', 'fs'), 'tp'), parts along dimension 0
There are 2 independent parts, one for each index of `grp`. A program takes and returns all parts, laid end to end along the dimension named above; an argument that names none is the same for every part. Nothing has to cross between parts.
All inputs are finite; a program needn't handle non-finite values.
Results may differ from a plain program's by a relative error of at most 0.017.
Values may be sent and summed in bfloat16 or wider, within the bound.
A program may use at most 64 MiB of HBM per device.

v0:
```python
import jax
import jax.numpy as jnp
from jax import lax
from jax.sharding import PartitionSpec as P

EPS = 1e-06


def rms_scale(values, gain_vec):
    mean_sq = jnp.mean(values * values, axis=-1, keepdims=True)
    return values * lax.rsqrt(mean_sq + EPS) * gain_vec.astype(jnp.float32)


def per_device(
    tokens,
    first_gain,
    u_proj,
    v_proj,
    group_gain,
    spatial,
    spatial_bias,
    mix_proj,
    second_gain,
    up_proj,
    down_proj,
):
    whole_rows = lax.all_gather(tokens, "tp", axis=1, tiled=True)
    row_count = whole_rows.shape[0]
    normed_rows = rms_scale(whole_rows.astype(jnp.float32), first_gain).astype(jnp.bfloat16)
    local_width = u_proj.shape[1]
    column_part = normed_rows
    u_pre = jnp.dot(
        column_part,
        lax.all_gather(u_proj, "fs", axis=0, tiled=True),
        preferred_element_type=jnp.float32,
    )
    v_pre = jnp.dot(
        column_part,
        lax.all_gather(v_proj, "fs", axis=0, tiled=True),
        preferred_element_type=jnp.float32,
    )
    u_act = jax.nn.gelu(u_pre).astype(jnp.bfloat16)
    local_groups = group_gain.shape[0]
    group_width = group_gain.shape[1]
    v_groups = jax.nn.gelu(v_pre).reshape(row_count, local_groups, group_width)
    v_normed = rms_scale(v_groups, group_gain).astype(jnp.bfloat16)
    block_len = spatial.shape[1]
    block_view = v_normed.reshape(row_count // block_len, block_len, local_groups, group_width)
    causal_mask = jnp.tril(jnp.ones((block_len, block_len), jnp.bool_))
    masked_weights = jnp.where(causal_mask[None], spatial, jnp.zeros_like(spatial))
    mixed_vals = jnp.einsum(
        "gts,nsgd->ntgd", masked_weights, block_view, preferred_element_type=jnp.float32
    )
    mixed_vals = mixed_vals + spatial_bias.astype(jnp.float32).T[None, :, :, None]
    gated_vals = (u_act.astype(jnp.float32) * mixed_vals.reshape(row_count, local_width)).astype(
        jnp.bfloat16
    )
    gated_whole = lax.all_gather(gated_vals, "tp", axis=1, tiled=True)
    column_part = gated_whole
    mix_vals = jnp.dot(
        column_part,
        lax.all_gather(mix_proj, "fs", axis=0, tiled=True),
        preferred_element_type=jnp.float32,
    )
    mid_stream = (tokens.astype(jnp.float32) + mix_vals).astype(jnp.bfloat16)
    mid_whole = lax.all_gather(mid_stream, "tp", axis=1, tiled=True)
    normed_two = rms_scale(mid_whole.astype(jnp.float32), second_gain).astype(jnp.bfloat16)
    column_part = normed_two
    pre_act = jnp.dot(
        column_part,
        lax.all_gather(up_proj, "fs", axis=0, tiled=True),
        preferred_element_type=jnp.float32,
    )
    hidden_act = jnp.square(jax.nn.relu(pre_act)).astype(jnp.bfloat16)
    down_terms = jnp.dot(
        hidden_act,
        lax.all_gather(down_proj, "fs", axis=1, tiled=True),
        preferred_element_type=jnp.float32,
    )
    down_sum = lax.psum_scatter(
        down_terms.astype(jnp.bfloat16), "tp", scatter_dimension=1, tiled=True
    ).astype(jnp.float32)
    return (mid_stream.astype(jnp.float32) + down_sum).astype(jnp.bfloat16)


def solution(mesh):
    return jax.shard_map(
        per_device,
        mesh=mesh,
        in_specs=(
            P(("grp", "fs"), "tp"),
            P(),
            P("fs", "tp"),
            P("fs", "tp"),
            P("tp", None),
            P("tp", None, None),
            P("tp", None),
            P("fs", "tp"),
            P(),
            P("fs", "tp"),
            P("tp", "fs"),
        ),
        out_specs=P(("grp", "fs"), "tp"),
        check_vma=False,
    )
```

profile of v0, /device:TPU:0, one launch (start us, length us, event | category | flops | bytes accessed | tf_op | source)
XLA Modules:
  0.0 520.2 jit_solution(6290348988835134259)
XLA Ops:
  6.5 0.7 all-gather.9.cloned.1.call-update
  7.3 0.7 all-gather.13.cloned.1.call-update
  8.1 0.7 all-gather.11.cloned.1.call-update
  9.4 0.7 convert_element_type.58
  11.4 22.8 %all-gather.9.cloned.1.call-done = bf16[512,2048]{1,0:T(8,128)(2,1)} async-done(((bf16[512,512]{1,0:T(8,128)(2,1)}), bf16[512,2048]{1,0:T(8,128)(2,1)}) %all-gather.9.cloned.1.call-update) | async-done | bytes 2097168 | tf_op jit(solution)/shard_map/all_gather | solution.py:27
  34.2 2.1 fusion
  36.3 27.5 %all-gather.13.cloned.1.call-done = bf16[2048,256]{1,0:T(8,128)(2,1)} async-done(((bf16[512,256]{1,0:T(8,128)(2,1)}), bf16[2048,256]{1,0:T(8,128)(2,1)}) %all-gather.13.cloned.1.call-update) | async-done | bytes 1048592 | tf_op jit(solution)/shard_map/all_gather | solution.py:39
  63.8 3.5 fusion.52
  68.3 1.3 reshape.52
  70.2 1.0 copy.26
  71.2 21.6 %all-gather.11.cloned.1.call-done = bf16[2048,256]{1,0:T(8,128)(2,1)} async-done(((bf16[512,256]{1,0:T(8,128)(2,1)}), bf16[2048,256]{1,0:T(8,128)(2,1)}) %all-gather.11.cloned.1.call-update) | async-done | bytes 1048592 | tf_op jit(solution)/shard_map/all_gather | solution.py:34
  92.8 2.9 fusion.33
  95.8 25.8 %all-gather.17.cloned.1.call-done = bf16[1024,512]{1,0:T(8,128)(2,1)} async-done(((bf16[256,512]{1,0:T(8,128)(2,1)}), bf16[1024,512]{1,0:T(8,128)(2,1)}) %all-gather.17.cloned.1.call-update) | async-done | bytes 1048592 | tf_op jit(solution)/shard_map/all_gather | solution.py:62
  121.6 17.6 %all-gather.15.cloned.1.call-done = bf16[512,1024]{1,0:T(8,128)(2,1)} async-done(((bf16[512,256]{1,0:T(8,128)(2,1)}), bf16[512,1024]{1,0:T(8,128)(2,1)}) %all-gather.15.cloned.1.call-update) | async-done | bytes 1048592 | tf_op jit(solution)/shard_map/all_gather | solution.py:58
  139.2 3.0 fusion.9
  142.3 0.7 all-gather.21.cloned.1.call-update
  143.1 0.7 all-gather.23.cloned.1.call-update
  143.9 21.1 %all-gather.19.cloned.1.call-done = bf16[512,2048]{1,0:T(8,128)(2,1)} async-done(((bf16[512,512]{1,0:T(8,128)(2,1)}), bf16[512,2048]{1,0:T(8,128)(2,1)}) %all-gather.19.cloned.1.call-update) | async-done | bytes 2097168 | tf_op jit(solution)/shard_map/all_gather | solution.py:66
  165.0 2.1 fusion.3
  167.1 149.1 %all-gather.21.cloned.1.call-done = bf16[2048,2048]{1,0:T(8,128)(2,1)} async-done(((bf16[512,2048]{1,0:T(8,128)(2,1)}), bf16[2048,2048]{1,0:T(8,128)(2,1)}) %all-gather.21.cloned.1.call-update) | async-done | bytes 8388624 | tf_op jit(solution)/shard_map/all_gather | solution.py:71
  316.2 149.4 %all-gather.23.cloned.1.call-done = bf16[2048,2048]{1,0:T(8,128)(2,1)} async-done(((bf16[2048,512]{1,0:T(8,128)(2,1)}), bf16[2048,2048]{1,0:T(8,128)(2,1)}) %all-gather.23.cloned.1.call-update) | async-done | bytes 8388624 | tf_op jit(solution)/shard_map/all_gather | solution.py:77
  465.6 16.6 %convolution_convert_fusion = bf16[512,2048]{1,0:T(8,128)(2,1)} fusion(bf16[2048,2048]{1,0:T(8,128)(2,1)} %all-gather.23.cloned.1.call-done, bf16[2048,2048]{1,0:T(8,128)(2,1)} %all-gather.21.cloned.1.call-done, bf16[512,2048]{1,0:T(8,128)(2,1)} %all-gather.19.cloned.1.call-done, f32[2048]{0:T(1024)S(1)} %convert_element_type.68, f32[512]{0:T(512)S(1)} %add_rsqrt_fusion.1), kind=kOutput, calls=%fused_computation.11 | convolution fusion | flops 8598323200 | bytes 20981760 | tf_op jit(solution)/shard_map/dot_general | solution.py:75
  482.2 29.5 %reduce-scatter.2.cloned.1.call-done = bf16[512,512]{1,0:T(8,128)(2,1)} async-done(((bf16[512,2048]{1,0:T(8,128)(2,1)}), bf16[512,512]{1,0:T(8,128)(2,1)}) %reduce-scatter.2.cloned.1.call-update) | async-done | bytes 524304 | tf_op jit(solution)/shard_map/reduce_scatter | solution.py:80
  511.7 2.0 add_convert_fusion
  (35 shorter events, 3.8 us)
Async XLA Ops:
  6.5 27.7 %all-gather.9.cloned.1.call-start = ((), (), s32[]{:S(2)}) async-start(), calls=%async_computation.1 | async-start | bytes 2621440 | tf_op jit(solution)/shard_map/all_gather | solution.py:27
  7.3 56.5 %all-gather.13.cloned.1.call-start = ((), (), s32[]{:S(2)}) async-start(), calls=%async_computation.3 | async-start | bytes 1310720 | tf_op jit(solution)/shard_map/all_gather | solution.py:39
  8.0 84.8 %all-gather.11.cloned.1.call-start = ((), (), s32[]{:S(2)}) async-start(), calls=%async_computation.2 | async-start | bytes 1310720 | tf_op jit(solution)/shard_map/all_gather | solution.py:34
  8.7 112.9 %all-gather.17.cloned.1.call-start = ((), (), s32[]{:S(2)}) async-start(), calls=%async_computation.5 | async-start | bytes 1310720 | tf_op jit(solution)/shard_map/all_gather | solution.py:62
  9.3 129.9 %all-gather.15.cloned.1.call-start = ((), (), s32[]{:S(2)}) async-start(), calls=%async_computation.4 | async-start | bytes 1310720 | tf_op jit(solution)/shard_map/all_gather | solution.py:58
  36.3 33.6 %copy-start.3 = (bf16[2,128,128]{2,1,0:T(8,128)(2,1)S(1)}, bf16[2,128,128]{2,1,0:T(8,128)(2,1)}, u32[]{:S(2)}) copy-start(bf16[2,128,128]{2,1,0:T(8,128)(2,1)} %param.16) | copy-start | bytes 196612
  67.3 25.5 %copy-start.1 = (bf16[512,2048]{1,0:T(8,128)(2,1)S(1)}, bf16[512,2048]{1,0:T(8,128)(2,1)}, u32[]{:S(2)}) copy-start(bf16[512,2048]{1,0:T(8,128)(2,1)} %all-gather.9.cloned.1.call-done) | copy-start | bytes 6291460
  70.2 69.1 %copy-start.2 = (bf16[512,512]{1,0:T(8,128)(2,1)S(1)}, bf16[512,512]{1,0:T(8,128)(2,1)}, u32[]{:S(2)}) copy-start(bf16[512,512]{1,0:T(8,128)(2,1)} %param.11) | copy-start | bytes 1572868
  95.7 48.1 %copy-start.4 = (bf16[2048]{0:T(1024)(128)(2,1)S(1)}, bf16[2048]{0:T(1024)(128)(2,1)}, u32[]{:S(2)}) copy-start(bf16[2048]{0:T(1024)(128)(2,1)} %param.19) | copy-start | bytes 12292
  95.7 69.3 %all-gather.19.cloned.1.call-start = ((), (), s32[]{:S(2)}) async-start(), calls=%async_computation.6 | async-start | bytes 2621440 | tf_op jit(solution)/shard_map/all_gather | solution.py:66
  142.3 173.9 %all-gather.21.cloned.1.call-start = ((), (), s32[]{:S(2)}) async-start(), calls=%async_computation.7 | async-start | bytes 10485760 | tf_op jit(solution)/shard_map/all_gather | solution.py:71
  143.0 322.6 %all-gather.23.cloned.1.call-start = ((), (), s32[]{:S(2)}) async-start(), calls=%async_computation.8 | async-start | bytes 10485760 | tf_op jit(solution)/shard_map/all_gather | solution.py:77
  143.8 367.9 %reduce-scatter.2.cloned.1.call-start = ((), (), s32[]{:S(2)}) async-start(), calls=%async_computation.9 | async-start | bytes 2621440 | tf_op jit(solution)/shard_map/reduce_scatter | solution.py:80
  167.1 344.6 %copy-start = (bf16[512,512]{1,0:T(8,128)(2,1)S(1)}, bf16[512,512]{1,0:T(8,128)(2,1)}, u32[]{:S(2)}) copy-start(bf16[512,512]{1,0:T(8,128)(2,1)} %fusion.9) | copy-start | bytes 1572868
Sparse Core Ops, SparseCore 0:
  8.9 25.2 all-gather.8
  35.8 27.9 all-gather.12
  65.4 27.3 all-gather.10
  94.2 27.3 all-gather.16
  123.0 16.1 all-gather.14
  142.4 22.5 all-gather.18
  166.6 149.6 all-gather.20
  317.8 147.7 all-gather.22
  482.3 29.3 reduce-scatter.1
where the time goes:
time: 521 us; the launch traced here: 520 us
  waiting for transfers between devices  469 us (90%)
  matrix products  26.3 us (5%)
  between operations  13.3 us (3%)
  other arithmetic  8.82 us (2%)
    all_gather x1, waiting for transfers between devices, per_device(): lax.all_gather(down_proj, 'fs', axis=1, tiled=True)  149 us
    all_gather x1, waiting for transfers between devices, per_device(): lax.all_gather(up_proj, 'fs', axis=0, tiled=True)  149 us
    reduce_scatter x1, waiting for transfers between devices, per_device(): lax.psum_scatter(down_terms.astype(jnp.bfloat16), 'tp', scatter_dimension...  29.5 us
    all_gather x1, waiting for transfers between devices, per_device(): lax.all_gather(v_proj, 'fs', axis=0, tiled=True)  27.5 us
    all_gather x1, waiting for transfers between devices, per_device(): lax.all_gather(mix_proj, 'fs', axis=0, tiled=True)  25.8 us
    all_gather x1, waiting for transfers between devices, per_device(): whole_rows = lax.all_gather(tokens, 'tp', axis=1, tiled=True)  22.8 us
    all_gather x1, waiting for transfers between devices, per_device(): lax.all_gather(u_proj, 'fs', axis=0, tiled=True)  21.6 us
    all_gather x1, waiting for transfers between devices, per_device(): mid_whole = lax.all_gather(mid_stream, 'tp', axis=1, tiled=True)  21.1 us
  transfers between devices with their start and end apart: 9, of which 9 were waited for; matrix products, arithmetic and copies ran while one was open for 3% of the time, Pallas kernels for 0%

commit v1 on v0

--- a/solution.py
+++ b/solution.py
@@ -68,7 +68,9 @@
     column_part = normed_two
     pre_act = jnp.dot(
         column_part,
-        lax.all_gather(up_proj, "fs", axis=0, tiled=True),
+        jnp.concatenate(
+            lax.all_to_all(jnp.stack([up_proj] * lax.axis_size("fs")), "fs", 0, 0), axis=0
+        ),
         preferred_element_type=jnp.float32,
     )
     hidden_act = jnp.square(jax.nn.relu(pre_act)).astype(jnp.bfloat16)

time: 521 us -> 527 us (1.012)
  starting transfers between devices: 0.31 us -> 6.35 us
    all_to_all x0 -> x1, waiting for transfers between devices: none -> 304 us  [per_device(): lax.all_to_all(jnp.stack([up_proj] * lax.axis_size('fs')), 'fs', 0, 0)]
    all_gather x1, waiting for transfers between devices: 149 us -> 0.01 us  [per_device(): lax.all_gather(down_proj, 'fs', axis=1, tiled=True)]
    all_gather x1 -> x0, waiting for transfers between devices: 149 us -> none  [per_device(): lax.all_gather(up_proj, 'fs', axis=0, tiled=True)]
    all_gather x1, waiting for transfers between devices: 21.1 us -> 11.5 us  [per_device(): mid_whole = lax.all_gather(mid_stream, 'tp', axis=1, tiled=True)]
    all_to_all x0 -> x1, starting transfers between devices: none -> 5.9 us  [per_device(): lax.all_to_all(jnp.stack([up_proj] * lax.axis_size('fs')), 'fs', 0, 0)]
  transfers between devices with their start and end apart: 9 -> 9, of which waited for: 9 -> 8; matrix products, arithmetic and copies ran while one was open for 3% -> 4% of each run, Pallas kernels for 0% -> 0%
where the time goes in v1:
time: 527 us; the launch traced here: 526 us
  waiting for transfers between devices  464 us (88%)
  matrix products  26.3 us (5%)
  between operations  13.6 us (3%)
  other arithmetic  8.82 us (2%)
  local copies, waits for them, and re-layouts  7.23 us (1%)
  starting transfers between devices  6.35 us (1%)
    all_to_all x1, waiting for transfers between devices, per_device(): lax.all_to_all(jnp.stack([up_proj] * lax.axis_size('fs')), 'fs', 0, 0)  304 us
    reduce_scatter x1, waiting for transfers between devices, per_device(): lax.psum_scatter(down_terms.astype(jnp.bfloat16), 'tp', scatter_dimension...  29.7 us
    all_gather x1, waiting for transfers between devices, per_device(): lax.all_gather(v_proj, 'fs', axis=0, tiled=True)  27.5 us
    all_gather x1, waiting for transfers between devices, per_device(): lax.all_gather(mix_proj, 'fs', axis=0, tiled=True)  25.8 us
    all_gather x1, waiting for transfers between devices, per_device(): whole_rows = lax.all_gather(tokens, 'tp', axis=1, tiled=True)  22.8 us
    all_gather x1, waiting for transfers between devices, per_device(): lax.all_gather(u_proj, 'fs', axis=0, tiled=True)  21.6 us
    all_gather x1, waiting for transfers between devices, per_device(): gated_whole = lax.all_gather(gated_vals, 'tp', axis=1, tiled=True)  17.6 us
    dot_general x1, matrix products, per_device(): jnp.dot(hidden_act, lax.all_gather(down_proj, 'fs', axis=1, tiled=True),...  16.6 us
  transfers between devices with their start and end apart: 9, of which 8 were waited for; matrix products, arithmetic and copies ran while one was open for 4% of the time, Pallas kernels for 0%

profile of v1, /device:TPU:0, one launch (start us, length us, event | category | flops | bytes accessed | tf_op | source)
XLA Modules:
  0.0 526.3 jit_solution(17791289159973319721)
XLA Ops:
  6.5 0.7 all-gather.8.cloned.1.call-update
  7.3 0.7 all-gather.12.cloned.1.call-update
  8.1 0.7 all-gather.10.cloned.1.call-update
  9.4 0.7 convert_element_type.58
  11.4 22.8 %all-gather.8.cloned.1.call-done = bf16[512,2048]{1,0:T(8,128)(2,1)} async-done(((bf16[512,512]{1,0:T(8,128)(2,1)}), bf16[512,2048]{1,0:T(8,128)(2,1)}) %all-gather.8.cloned.1.call-update) | async-done | bytes 2097168 | tf_op jit(solution)/shard_map/all_gather | solution.py:27
  34.2 2.1 fusion
  36.3 27.5 %all-gather.12.cloned.1.call-done = bf16[2048,256]{1,0:T(8,128)(2,1)} async-done(((bf16[512,256]{1,0:T(8,128)(2,1)}), bf16[2048,256]{1,0:T(8,128)(2,1)}) %all-gather.12.cloned.1.call-update) | async-done | bytes 1048592 | tf_op jit(solution)/shard_map/all_gather | solution.py:39
  63.8 3.5 fusion.52
  68.3 1.3 reshape.57
  70.2 1.0 copy.26
  71.2 21.6 %all-gather.10.cloned.1.call-done = bf16[2048,256]{1,0:T(8,128)(2,1)} async-done(((bf16[512,256]{1,0:T(8,128)(2,1)}), bf16[2048,256]{1,0:T(8,128)(2,1)}) %all-gather.10.cloned.1.call-update) | async-done | bytes 1048592 | tf_op jit(solution)/shard_map/all_gather | solution.py:34
  92.8 2.9 fusion.33
  95.7 25.8 %all-gather.16.cloned.1.call-done = bf16[1024,512]{1,0:T(8,128)(2,1)} async-done(((bf16[256,512]{1,0:T(8,128)(2,1)}), bf16[1024,512]{1,0:T(8,128)(2,1)}) %all-gather.16.cloned.1.call-update) | async-done | bytes 1048592 | tf_op jit(solution)/shard_map/all_gather | solution.py:62
  121.6 17.6 %all-gather.14.cloned.1.call-done = bf16[512,1024]{1,0:T(8,128)(2,1)} async-done(((bf16[512,256]{1,0:T(8,128)(2,1)}), bf16[512,1024]{1,0:T(8,128)(2,1)}) %all-gather.14.cloned.1.call-update) | async-done | bytes 1048592 | tf_op jit(solution)/shard_map/all_gather | solution.py:58
  139.2 3.0 fusion.9
  142.3 4.3 stack.2
  146.6 5.9 %all-to-all-start = ((bf16[4,512,2048]{2,1,0:T(8,128)(2,1)}), bf16[4,512,2048]{2,1,0:T(8,128)(2,1)}, u32[]{:S(2)}, u32[]{:S(2)}) async-start(bf16[4,512,2048]{2,1,0:T(8,128)(2,1)} %stack.2), calls=%async_computation | async-start | bytes 16777216 | tf_op jit(solution)/shard_map/all_to_all | solution.py:72
  152.6 0.7 all-gather.20.cloned.1.call-update
  153.5 11.5 %all-gather.18.cloned.1.call-done = bf16[512,2048]{1,0:T(8,128)(2,1)} async-done(((bf16[512,512]{1,0:T(8,128)(2,1)}), bf16[512,2048]{1,0:T(8,128)(2,1)}) %all-gather.18.cloned.1.call-update) | async-done | bytes 2097168 | tf_op jit(solution)/shard_map/all_gather | solution.py:66
  165.0 2.1 fusion.3
  167.1 304.0 %all-to-all-done = bf16[4,512,2048]{2,1,0:T(8,128)(2,1)} async-done(((bf16[4,512,2048]{2,1,0:T(8,128)(2,1)}), bf16[4,512,2048]{2,1,0:T(8,128)(2,1)}, u32[]{:S(2)}, u32[]{:S(2)}) %all-to-all-start) | async-done | bytes 8388640 | tf_op jit(solution)/shard_map/all_to_all | solution.py:72
  471.1 16.6 %convolution_convert_fusion = bf16[512,2048]{1,0:T(8,128)(2,1)} fusion(bf16[2048,2048]{1,0:T(8,128)(2,1)} %all-gather.20.cloned.1.call-done, bf16[2048,2048]{1,0:T(8,128)(2,1)} %bitcast.5, bf16[512,2048]{1,0:T(8,128)(2,1)} %all-gather.18.cloned.1.call-done, f32[2048]{0:T(1024)S(1)} %convert_element_type.68, f32[512]{0:T(512)S(1)} %add_rsqrt_fusion.1), kind=kOutput, calls=%fused_computation.11 | convolution fusion | flops 8598323200 | bytes 20981760 | tf_op jit(solution)/shard_map/dot_general | solution.py:77
  487.8 29.7 %reduce-scatter.2.cloned.1.call-done = bf16[512,512]{1,0:T(8,128)(2,1)} async-done(((bf16[512,2048]{1,0:T(8,128)(2,1)}), bf16[512,512]{1,0:T(8,128)(2,1)}) %reduce-scatter.2.cloned.1.call-update) | async-done | bytes 524304 | tf_op jit(solution)/shard_map/reduce_scatter | solution.py:82
  517.4 2.0 add_convert_fusion
  (37 shorter events, 3.9 us)
Async XLA Ops:
  6.5 27.7 %all-gather.8.cloned.1.call-start = ((), (), s32[]{:S(2)}) async-start(), calls=%async_computation.2 | async-start | bytes 2621440 | tf_op jit(solution)/shard_map/all_gather | solution.py:27
  7.3 56.5 %all-gather.12.cloned.1.call-start = ((), (), s32[]{:S(2)}) async-start(), calls=%async_computation.4 | async-start | bytes 1310720 | tf_op jit(solution)/shard_map/all_gather | solution.py:39
  8.0 84.8 %all-gather.10.cloned.1.call-start = ((), (), s32[]{:S(2)}) async-start(), calls=%async_computation.3 | async-start | bytes 1310720 | tf_op jit(solution)/shard_map/all_gather | solution.py:34
  8.7 112.8 %all-gather.16.cloned.1.call-start = ((), (), s32[]{:S(2)}) async-start(), calls=%async_computation.6 | async-start | bytes 1310720 | tf_op jit(solution)/shard_map/all_gather | solution.py:62
  9.3 129.9 %all-gather.14.cloned.1.call-start = ((), (), s32[]{:S(2)}) async-start(), calls=%async_computation.5 | async-start | bytes 1310720 | tf_op jit(solution)/shard_map/all_gather | solution.py:58
  36.3 33.6 %copy-start.4 = (bf16[2,128,128]{2,1,0:T(8,128)(2,1)S(1)}, bf16[2,128,128]{2,1,0:T(8,128)(2,1)}, u32[]{:S(2)}) copy-start(bf16[2,128,128]{2,1,0:T(8,128)(2,1)} %param.16) | copy-start | bytes 196612
  67.3 25.5 %copy-start.2 = (bf16[512,2048]{1,0:T(8,128)(2,1)S(1)}, bf16[512,2048]{1,0:T(8,128)(2,1)}, u32[]{:S(2)}) copy-start(bf16[512,2048]{1,0:T(8,128)(2,1)} %all-gather.8.cloned.1.call-done) | copy-start | bytes 6291460
  70.2 69.1 %copy-start.3 = (bf16[512,512]{1,0:T(8,128)(2,1)S(1)}, bf16[512,512]{1,0:T(8,128)(2,1)}, u32[]{:S(2)}) copy-start(bf16[512,512]{1,0:T(8,128)(2,1)} %param.11) | copy-start | bytes 1572868
  95.7 46.6 %copy-start = (bf16[512,2048]{1,0:T(8,128)(2,1)S(1)}, bf16[512,2048]{1,0:T(8,128)(2,1)}, u32[]{:S(2)}) copy-start(bf16[512,2048]{1,0:T(8,128)(2,1)} %param.20) | copy-start | bytes 6291460
  95.7 69.3 %all-gather.18.cloned.1.call-start = ((), (), s32[]{:S(2)}) async-start(), calls=%async_computation.7 | async-start | bytes 2621440 | tf_op jit(solution)/shard_map/all_gather | solution.py:66
  146.6 6.9 %copy-start.5 = (bf16[2048]{0:T(1024)(128)(2,1)S(1)}, bf16[2048]{0:T(1024)(128)(2,1)}, u32[]{:S(2)}) copy-start(bf16[2048]{0:T(1024)(128)(2,1)} %param.19) | copy-start | bytes 12292
  146.6 324.5 %all-to-all-start = ((bf16[4,512,2048]{2,1,0:T(8,128)(2,1)}), bf16[4,512,2048]{2,1,0:T(8,128)(2,1)}, u32[]{:S(2)}, u32[]{:S(2)}) async-start(bf16[4,512,2048]{2,1,0:T(8,128)(2,1)} %stack.2), calls=%async_computation | async-start | bytes 16777216 | tf_op jit(solution)/shard_map/all_to_all | solution.py:72
  152.5 318.6 %all-gather.20.cloned.1.call-start = ((), (), s32[]{:S(2)}) async-start(), calls=%async_computation.8 | async-start | bytes 10485760 | tf_op jit(solution)/shard_map/all_gather | solution.py:79
  153.3 364.2 %reduce-scatter.2.cloned.1.call-start = ((), (), s32[]{:S(2)}) async-start(), calls=%async_computation.9 | async-start | bytes 2621440 | tf_op jit(solution)/shard_map/reduce_scatter | solution.py:82
  471.1 46.3 %copy-start.1 = (bf16[512,512]{1,0:T(8,128)(2,1)S(1)}, bf16[512,512]{1,0:T(8,128)(2,1)}, u32[]{:S(2)}) copy-start(bf16[512,512]{1,0:T(8,128)(2,1)} %fusion.9) | copy-start | bytes 1572868
Sparse Core Ops, SparseCore 0:
  8.9 25.2 all-gather.7
  35.8 27.9 all-gather.11
  65.4 27.3 all-gather.9
  94.2 27.3 all-gather.15
  123.0 16.1 all-gather.13
  142.4 22.5 all-gather.17
  166.6 283.2 all-gather.19
  487.9 29.5 reduce-scatter.1
